TPU v7x, 32 devices: a whole 2x2x4 slice. The times are simulated.
32 devices in a mesh: sp: 8 (over z, core), tp: 4 (over y, x).
Axes of the slice: x: 2, y: 2, z: 4, core: 2. Of those that a mesh axis runs over, the one named last changes fastest.
Arguments:
- queries: bfloat16 [2048, 2048], P('sp', 'tp'), may hold values from -6 to 6
- keys: bfloat16 [2048, 1024], P('sp', 'tp'), may hold values from -6 to 6
- values: bfloat16 [2048, 1024], P('sp', 'tp'), may hold values from -6 to 6
- sink_logit: float32 [32], P('tp'), may hold values from -1 to 6
- out_weight: bfloat16 [2048, 2048], P(None, 'tp'), may hold values from -0.125 to 0.125
- residual: bfloat16 [2048, 2048], P(('sp', 'tp')), may hold values from -1.796875 to 1.796875
- norm_gain: float32 [2048], replicated, may hold values from 0.1 to 1.9
- routes: int32 [2048, 2], P(('sp', 'tp')), may hold values from 0 to 7, all different within a row; in each aligned block of 64 rows (0 to 63, 64 to 127, ...) at most 32 rows name the same one
- route_weights: float32 [2048, 2], P(('sp', 'tp')), may hold values from 0.2 to 1
- gate_weight: bfloat16 [8, 2048, 5120], P('sp', None, 'tp'), may hold values from -0.125 to 0.125
- up_weight: bfloat16 [8, 2048, 5120], P('sp', None, 'tp'), may hold values from -0.125 to 0.125
- down_weight: bfloat16 [8, 5120, 2048], P('sp', 'tp'), may hold values from -0.078125 to 0.078125
Outputs:
- mixed: bfloat16 [2048, 2048], P(('sp', 'tp'))
Inputs may be any that keep to these rules, and one draw needn't show every extreme that they name: `routes`: each row names two different experts. Among the rows of one device no expert is named more than 32 times, and in every draw some expert is named exactly 32 times by the rows of some device.
All inputs are finite; a program needn't handle non-finite values.
Results may differ from a plain program's by a relative error of at most 0.018.
Values may be sent and summed in bfloat16 or wider, within the bound.
A program may use at most 64 MiB of HBM per device.

v0:
```python
import jax
import jax.numpy as jnp
from jax import lax
from jax.sharding import PartitionSpec as P

HEADS = 32
KV_HEADS = 16
HEAD = 64
WINDOW = 128


EPS = 1e-06
NEGATIVE = -1e30


def with_halo(block, sides, width):
    for axis, dim in sides:
        count = lax.axis_size(axis)
        forward = [(i, i + 1) for i in range(count - 1)]
        backward = [(target, source) for source, target in forward]
        low = lax.ppermute(
            lax.slice_in_dim(block, block.shape[dim] - width, None, axis=dim), axis, forward
        )
        high = lax.ppermute(lax.slice_in_dim(block, 0, width, axis=dim), axis, backward)
        block = jnp.concatenate([low, block, high], axis=dim)
    return block


def make_band(extended, length):
    blocks = length // WINDOW
    pieces = [
        lax.slice_in_dim(extended, offset * WINDOW, offset * WINDOW + length, axis=0).reshape(
            blocks, WINDOW, -1
        )
        for offset in range(3)
    ]
    return jnp.concatenate(pieces, axis=1)


def attend_local(queries, keys, values, sink_logit):
    length = queries.shape[0]
    groups = keys.shape[1] // HEAD
    repeat = HEADS // KV_HEADS
    blocks = length // WINDOW
    joined = jnp.concatenate([keys, values], axis=1)
    extended = with_halo(joined, (("sp", 0),), WINDOW)
    banded = make_band(extended, length)
    key_band = banded[..., : groups * HEAD].reshape(blocks, 3 * WINDOW, groups, HEAD)
    value_band = banded[..., groups * HEAD :].reshape(blocks, 3 * WINDOW, groups, HEAD)
    query_blocks = queries.reshape(blocks, WINDOW, groups, repeat, HEAD)
    scores = jnp.einsum(
        "nqgrd,nkgd->ngrqk", query_blocks, key_band, preferred_element_type=jnp.float32
    ) * HEAD ** (-0.5)
    near = jnp.abs(jnp.arange(WINDOW)[:, None] + WINDOW - jnp.arange(3 * WINDOW)[None, :]) <= WINDOW
    first_token = lax.axis_index("sp") * length
    key_pos = (
        first_token + (jnp.arange(blocks)[:, None] - 1) * WINDOW + jnp.arange(3 * WINDOW)[None, :]
    )
    inside = (key_pos >= 0) & (key_pos < length * lax.axis_size("sp"))
    valid = near[None, None, None, :, :] & inside[:, None, None, None, :]
    sinks = sink_logit.reshape(1, groups, repeat, 1, 1)
    masked = jnp.where(valid, scores, NEGATIVE)
    top = jnp.maximum(jnp.max(masked, axis=-1, keepdims=True), sinks)
    probs = jnp.exp(masked - top)
    denom = jnp.sum(probs, axis=-1, keepdims=True) + jnp.exp(sinks - top)
    weights = (probs / denom).astype(jnp.bfloat16)
    output = jnp.einsum(
        "ngrqk,nkgd->nqgrd", weights, value_band, preferred_element_type=jnp.float32
    )
    return output.astype(jnp.bfloat16).reshape(length, groups * repeat * HEAD)


def local(
    queries,
    keys,
    values,
    sink_logit,
    out_weight,
    residual,
    norm_gain,
    routes,
    route_weights,
    gate_weight,
    up_weight,
    down_weight,
):
    attention = attend_local(queries, keys, values, sink_logit)
    columns = jnp.dot(
        lax.all_gather(attention, "tp", axis=1, tiled=True),
        out_weight,
        preferred_element_type=jnp.float32,
    )
    projected = lax.all_to_all(
        columns.astype(jnp.bfloat16), "tp", split_axis=0, concat_axis=1, tiled=True
    )
    hidden_state = residual.astype(jnp.float32) + projected.astype(jnp.float32)
    inverse = lax.rsqrt(jnp.mean(hidden_state * hidden_state, axis=-1, keepdims=True) + EPS)
    normed = (hidden_state * inverse * norm_gain).astype(jnp.bfloat16)
    sp_count = lax.axis_size("sp")
    tok_rows = residual.shape[0]
    width = residual.shape[1]
    capacity = max(2, 4 * tok_rows // sp_count)
    slot_total = sp_count * capacity
    expert_ids = routes.reshape(-1)
    onehot = (expert_ids[:, None] == jnp.arange(sp_count, dtype=jnp.int32)[None, :]).astype(
        jnp.int32
    )
    earlier = jnp.cumsum(onehot, axis=0) - onehot
    rank = jnp.sum(earlier * onehot, axis=1)
    slots = expert_ids * capacity + rank
    placing = (slots[:, None] == jnp.arange(slot_total, dtype=jnp.int32)[None, :]).astype(
        jnp.bfloat16
    )
    placing = placing.reshape(tok_rows, 2, slot_total)
    first_place = placing[:, 0]
    second_place = placing[:, 1]
    sending = jnp.einsum(
        "ts,td->sd", first_place + second_place, normed, preferred_element_type=jnp.float32
    )
    sending = sending.astype(jnp.bfloat16).reshape(sp_count, capacity, width)
    piece = lax.all_gather(
        lax.all_to_all(sending, "sp", split_axis=0, concat_axis=0, tiled=True),
        "tp",
        axis=0,
        tiled=True,
    )
    flat = piece.reshape(-1, piece.shape[-1])
    gate = jnp.dot(flat, gate_weight[0], preferred_element_type=jnp.float32)
    upward = jnp.dot(flat, up_weight[0], preferred_element_type=jnp.float32)
    hidden = (jax.nn.silu(gate) * upward).astype(jnp.bfloat16)
    partial_value = jnp.dot(hidden, down_weight[0], preferred_element_type=jnp.float32)
    partial_value = partial_value.reshape(piece.shape[:-1] + (down_weight.shape[-1],))
    returned = lax.all_to_all(
        lax.psum_scatter(partial_value.astype(jnp.bfloat16), "tp", scatter_dimension=0, tiled=True),
        "sp",
        split_axis=0,
        concat_axis=0,
        tiled=True,
    )
    gathered_back = returned.reshape(slot_total, width)
    first_pick = jnp.dot(first_place, gathered_back, preferred_element_type=jnp.float32)
    second_pick = jnp.dot(second_place, gathered_back, preferred_element_type=jnp.float32)
    mixture = route_weights[:, 0:1] * first_pick + route_weights[:, 1:2] * second_pick
    return (hidden_state + mixture).astype(jnp.bfloat16)


def solution(mesh):
    in_specs = (
        P("sp", "tp"),
        P("sp", "tp"),
        P("sp", "tp"),
        P("tp"),
        P(None, "tp"),
        P(("sp", "tp"), None),
        P(),
        P(("sp", "tp"), None),
        P(("sp", "tp"), None),
        P("sp", None, "tp"),
        P("sp", None, "tp"),
        P("sp", "tp", None),
    )
    out_specs = P(("sp", "tp"), None)
    return jax.shard_map(local, mesh=mesh, in_specs=in_specs, out_specs=out_specs, check_vma=False)
```

profile of v0, /device:TPU:0, one launch (start us, length us, event | category | flops | bytes accessed | tf_op | source)
XLA Modules:
  0.0 268.1 jit_solution(7856770385104215598)
XLA Ops:
  6.5 1.1 constant_dynamic-update-slice_fusion.1
  7.6 0.9 constant_dynamic-update-slice_fusion
  8.5 0.7 fusion.31
  9.2 3.0 %collective-permute-start = (bf16[128,512]{1,0:T(8,128)(2,1)}, bf16[128,512]{1,0:T(8,128)(2,1)}, u32[]{:S(2)}, u32[]{:S(2)}) collective-permute-start(bf16[128,512]{1,0:T(8,128)(2,1)} %get-tuple-element.9), channel_id=1, source_target_pairs={{0,4},{4,8},{8,12},{12,16},{16,20},{20,24},{24,28},{1,5},{5,9},{9,... | collective-permute-start | bytes 393224 | tf_op jit(solution)/shard_map/ppermute | solution.py:21
  12.2 1.3 collective-permute-start.1
  13.9 1.3 reshape.167
  15.1 0.7 max.18
  16.1 1.1 collective-permute-done.1
  17.1 1.7 pad_maximum_fusion.2
  18.9 1.1 copy.46
  20.0 0.8 copy.48
  20.8 1.1 pad_maximum_fusion
  22.0 0.7 fusion.12
  22.8 0.7 fusion.11
  23.5 1.0 fusion.18
  24.8 0.7 copy.68
  26.5 29.1 %all-gather.3.cloned.1.call-done = bf16[256,2048]{0,1:T(8,128)(2,1)} async-done(((bf16[256,512]{0,1:T(8,128)(2,1)}), bf16[256,2048]{0,1:T(8,128)(2,1)}) %all-gather.3.cloned.1.call-update) | async-done | bytes 1048592 | tf_op jit(solution)/shard_map/all_gather | solution.py:89
  55.6 2.7 convolution_convert_fusion.1
  58.2 3.4 %all-to-all-start = ((bf16[4,64,512]{2,1,0:T(8,128)(2,1)}), bf16[4,64,512]{2,1,0:T(8,128)(2,1)S(1)}, u32[]{:S(2)}, u32[]{:S(2)}) async-start(bf16[4,64,512]{2,1,0:T(8,128)(2,1)} %bitcast.11), calls=%async_computation | async-start | bytes 524288 | tf_op jit(solution)/shard_map/all_to_all | solution.py:93
  61.8 5.3 %all-to-all-done = bf16[4,64,512]{2,1,0:T(8,128)(2,1)S(1)} async-done(((bf16[4,64,512]{2,1,0:T(8,128)(2,1)}), bf16[4,64,512]{2,1,0:T(8,128)(2,1)S(1)}, u32[]{:S(2)}, u32[]{:S(2)}) %all-to-all-start) | async-done | bytes 262176 | tf_op jit(solution)/shard_map/all_to_all | solution.py:93
  67.4 0.6 copy-done.1
  68.0 0.5 convolution_convert_fusion
  68.5 31.1 %all_to_all.23 = bf16[8,32,2048]{2,1,0:T(8,128)(2,1)} all-to-all(bf16[8,32,2048]{2,1,0:T(8,128)(2,1)S(1)} %bitcast.85), channel_id=1, replica_groups=mesh['sp'=8,'tp'=4] {'sp'}, dimensions={0} | all-to-all | bytes 2097152 | tf_op jit(solution)/shard_map/all_to_all | solution.py:122
  99.8 50.3 %all-gather.5.cloned.1.call-done = bf16[32,32,2048]{2,1,0:T(8,128)(2,1)} async-done(((bf16[8,32,2048]{2,1,0:T(8,128)(2,1)}), bf16[32,32,2048]{2,1,0:T(8,128)(2,1)}) %all-gather.5.cloned.1.call-update) | async-done | bytes 4194320 | tf_op jit(solution)/shard_map/all_gather | solution.py:121
  150.1 9.0 %fusion.2 = f32[1024,1280]{1,0:T(8,128)S(1)} fusion(bf16[1024,2048]{1,0:T(8,128)(2,1)} %bitcast.95, bf16[1,2048,1280]{2,1,0:T(8,128)(2,1)} %param.22), kind=kOutput, calls=%fused_computation.2 | convolution fusion | flops 5368709120 | bytes 14680064 | tf_op jit(solution)/shard_map/dot_general | solution.py:129
  159.2 8.9 %multiply_convert_fusion = bf16[1024,1280]{1,0:T(8,128)(2,1)S(1)} fusion(f32[1024,1280]{1,0:T(8,128)S(1)} %fusion.2, bf16[1024,2048]{1,0:T(8,128)(2,1)S(1)} %bitcast.96, bf16[1,2048,1280]{2,1,0:T(8,128)(2,1)} %param.21), kind=kOutput, calls=%fused_computation.6 | convolution fusion | flops 5376573440 | bytes 17301504 | tf_op jit(solution)/shard_map/dot_general | solution.py:128
  168.1 7.1 %fusion.8 = bf16[32,32,2048]{2,1,0:T(8,128)(2,1)} fusion(bf16[32,32,1280]{2,1,0:T(8,128)(2,1)S(1)} %bitcast.97, bf16[1,1280,2048]{2,1,0:T(8,128)(2,1)S(1)} %bitcast.94), kind=kOutput, calls=%fused_computation.7 | convolution fusion | flops 5370806272 | bytes 12058624 | tf_op jit(solution)/shard_map/dot_general | solution.py:131
  175.3 52.8 %reduce-scatter.2.cloned.1.call-done = bf16[8,32,2048]{2,1,0:T(8,128)(2,1)} async-done(((bf16[32,32,2048]{2,1,0:T(8,128)(2,1)}), bf16[8,32,2048]{2,1,0:T(8,128)(2,1)}) %reduce-scatter.2.cloned.1.call-update) | async-done | bytes 1048592 | tf_op jit(solution)/shard_map/reduce_scatter | solution.py:134
  228.1 4.6 %all-to-all-start.2 = ((bf16[8,32,2048]{2,1,0:T(8,128)(2,1)}), bf16[8,32,2048]{2,1,0:T(8,128)(2,1)S(1)}, u32[]{:S(2)}, u32[]{:S(2)}) async-start(bf16[8,32,2048]{2,1,0:T(8,128)(2,1)} %reduce-scatter.2.cloned.1.call-done), calls=%async_computation.3 | async-start | bytes 2097152 | tf_op jit(solution)/shard_map/all_to_all | solution.py:133
  232.7 26.5 %all-to-all-done.2 = bf16[8,32,2048]{2,1,0:T(8,128)(2,1)S(1)} async-done(((bf16[8,32,2048]{2,1,0:T(8,128)(2,1)}), bf16[8,32,2048]{2,1,0:T(8,128)(2,1)S(1)}, u32[]{:S(2)}, u32[]{:S(2)}) %all-to-all-start.2) | async-done | bytes 1048608 | tf_op jit(solution)/shard_map/all_to_all | solution.py:133
  259.2 0.3 convolution_multiply_fusion.1
  259.5 2.1 fusion.15
  (49 shorter events, 2.6 us)
Async XLA Ops:
  6.5 49.0 %copy-start = (bf16[2048,512]{1,0:T(8,128)(2,1)S(1)}, bf16[2048,512]{1,0:T(8,128)(2,1)}, u32[]{:S(2)}) copy-start(bf16[2048,512]{1,0:T(8,128)(2,1)} %param.16) | copy-start | bytes 6291460
  6.5 49.0 %all-gather.3.cloned.1.call-start = ((), (), s32[]{:S(2)}) async-start(), calls=%async_computation.4 | async-start | bytes 1310720 | tf_op jit(solution)/shard_map/all_gather | solution.py:89
  9.2 6.9 %collective-permute-start = (bf16[128,512]{1,0:T(8,128)(2,1)}, bf16[128,512]{1,0:T(8,128)(2,1)}, u32[]{:S(2)}, u32[]{:S(2)}) collective-permute-start(bf16[128,512]{1,0:T(8,128)(2,1)} %get-tuple-element.9), channel_id=1, source_target_pairs={{0,4},{4,8},{8,12},{12,16},{16,20},{20,24},{24,28},{1,5},{5,9},{9,... | collective-permute-start | bytes 393224 | tf_op jit(solution)/shard_map/ppermute | solution.py:21
  12.2 4.9 %collective-permute-start.1 = (bf16[128,512]{1,0:T(8,128)(2,1)S(1)}, bf16[128,512]{1,0:T(8,128)(2,1)}, u32[]{:S(2)}, u32[]{:S(2)}) collective-permute-start(bf16[128,512]{1,0:T(8,128)(2,1)S(1)} %get-tuple-element.10), channel_id=1, source_target_pairs={{4,0},{8,4},{12,8},{16,12},{20,16},{24,20},{28,24},{5,1},{9,5},{13... | collective-permute-start | bytes 393224 | tf_op jit(solution)/shard_map/ppermute | solution.py:24
  23.5 2.0 copy-start.4
  26.4 40.8 %copy-start.2 = (bf16[64,2048]{1,0:T(8,128)(2,1)S(1)}, bf16[64,2048]{1,0:T(8,128)(2,1)}, u32[]{:S(2)}) copy-start(bf16[64,2048]{1,0:T(8,128)(2,1)} %param.17) | copy-start | bytes 786436
  26.4 41.6 %copy-start.3 = (f32[2048]{0:T(1024)S(1)}, f32[2048]{0:T(1024)}, u32[]{:S(2)}) copy-start(f32[2048]{0:T(1024)} %param.18) | copy-start | bytes 24580
  58.2 8.9 %all-to-all-start = ((bf16[4,64,512]{2,1,0:T(8,128)(2,1)}), bf16[4,64,512]{2,1,0:T(8,128)(2,1)S(1)}, u32[]{:S(2)}, u32[]{:S(2)}) async-start(bf16[4,64,512]{2,1,0:T(8,128)(2,1)} %bitcast.11), calls=%async_computation | async-start | bytes 524288 | tf_op jit(solution)/shard_map/all_to_all | solution.py:93
  61.6 88.5 %all-gather.5.cloned.1.call-start = ((), (), s32[]{:S(2)}) async-start(), calls=%async_computation.5 | async-start | bytes 5242880 | tf_op jit(solution)/shard_map/all_gather | solution.py:121
  67.2 0.8 copy-start.1
  99.6 128.4 %reduce-scatter.2.cloned.1.call-start = ((), (), s32[]{:S(2)}) async-start(), calls=%async_computation.6 | async-start | bytes 5242880 | tf_op jit(solution)/shard_map/reduce_scatter | solution.py:134
  150.1 9.0 %copy-start.6 = (bf16[32,32,2048]{2,1,0:T(8,128)(2,1)S(1)}, bf16[32,32,2048]{2,1,0:T(8,128)(2,1)}, u32[]{:S(2)}) copy-start(bf16[32,32,2048]{2,1,0:T(8,128)(2,1)} %all-gather.5.cloned.1.call-done) | copy-start | bytes 12582916
  150.1 18.0 %slice-start = ((s8[5242880]{0:T(1024)(128)(4,1)}), s8[4194304]{0:T(1024)(128)(4,1)S(1)}, s32[]{:S(2)}) async-start(s8[5242880]{0:T(1024)(128)(4,1)} %bitcast.93), calls=%async_computation.7 | async-start | bytes 8388608
  159.2 8.9 %slice-start.1 = ((s8[5242880]{0:T(1024)(128)(4,1)}), s8[1048576]{0:T(1024)(128)(4,1)S(1)}, s32[]{:S(2)}) async-start(s8[5242880]{0:T(1024)(128)(4,1)} %bitcast.93), calls=%async_computation.8 | async-start | bytes 2097152
  175.2 57.4 %copy-start.5 = (f32[64,2]{0,1:T(2,128)S(1)}, f32[64,2]{0,1:T(2,128)}, u32[]{:S(2)}) copy-start(f32[64,2]{0,1:T(2,128)} %param.20) | copy-start | bytes 1540
  228.1 31.2 %all-to-all-start.2 = ((bf16[8,32,2048]{2,1,0:T(8,128)(2,1)}), bf16[8,32,2048]{2,1,0:T(8,128)(2,1)S(1)}, u32[]{:S(2)}, u32[]{:S(2)}) async-start(bf16[8,32,2048]{2,1,0:T(8,128)(2,1)} %reduce-scatter.2.cloned.1.call-done), calls=%async_computation.3 | async-start | bytes 2097152 | tf_op jit(solution)/shard_map/all_to_all | solution.py:133
Sparse Core Ops, SparseCore 0:
  25.6 29.8 all-gather.2
  99.7 50.3 all-gather.4
  175.4 52.6 reduce-scatter.1
where the time goes:
time: 269 us; the launch traced here: 268 us
  waiting for transfers between devices  165 us (61%)
  matrix products  32.2 us (12%)
  blocking collectives  31.1 us (12%)
  between operations  13.4 us (5%)
  starting transfers between devices  12.6 us (5%)
  local copies, waits for them, and re-layouts  9.03 us (3%)
  other arithmetic  4.66 us (2%)
    reduce_scatter x1, waiting for transfers between devices, local(): lax.psum_scatter(partial_value.astype(jnp.bfloat16), 'tp', scatter_dimens...  52.8 us
    all_gather x1, waiting for transfers between devices, local(): lax.all_gather(lax.all_to_all(sending, 'sp', split_axis=0, concat_axis=0,...  50.3 us
    all_to_all x1, blocking collectives, local(): lax.all_to_all(sending, 'sp', split_axis=0, concat_axis=0, tiled=True)  31.1 us
    all_gather x1, waiting for transfers between devices, local(): lax.all_gather(attention, 'tp', axis=1, tiled=True)  29.1 us
    all_to_all x1, waiting for transfers between devices, local(): lax.all_to_all(lax.psum_scatter(partial_value.astype(jnp.bfloat16), 'tp',...  26.5 us
    dot_general x1, matrix products, local(): upward = jnp.dot(flat, up_weight[0], preferred_element_type=jnp.float32)  9.03 us
    dot_general x1, matrix products, local(): gate = jnp.dot(flat, gate_weight[0], preferred_element_type=jnp.float32)  8.92 us
    dot_general x1, matrix products, local(): jnp.dot(hidden, down_weight[0], preferred_element_type=jnp.float32)  7.12 us
  transfers between devices with their start and end apart: 7, of which 6 were waited for; matrix products, arithmetic and copies ran while one was open for 1% of the time, Pallas kernels for 0%

commit v1 on v0

--- a/solution.py
+++ b/solution.py
@@ -1,6 +1,10 @@
+import functools
+
 import jax
 import jax.numpy as jnp
 from jax import lax
+from jax.experimental import pallas as pl
+from jax.experimental.pallas import tpu as pltpu
 from jax.sharding import PartitionSpec as P
 
 HEADS = 32
@@ -11,6 +15,208 @@
 
 EPS = 1e-06
 NEGATIVE = -1e30
+MESH = pl.DeviceIdType.MESH
+
+
+def plane():
+    t = lax.axis_index("tp")
+    tx = t + 1 - 2 * lax.rem(t, 2)
+    ty = lax.rem(t + 2, 4)
+    return t, tx, ty, 3 - t
+
+
+def greet(devices):
+    barrier = pltpu.get_barrier_semaphore()
+    for device in devices:
+        pl.semaphore_signal(barrier, inc=1, device_id=device, device_id_type=MESH)
+    pl.semaphore_wait(barrier, len(devices))
+
+
+def remote(src, dst, send, recv, device):
+    return pltpu.make_async_remote_copy(
+        src_ref=src,
+        dst_ref=dst,
+        send_sem=send,
+        recv_sem=recv,
+        device_id=device,
+        device_id_type=MESH,
+    )
+
+
+def dispatch_kernel(n, send_ref, out_ref, zs, zr, xs, xr, ys, yr, xhs, xhr, yhs, yhr):
+    s = lax.axis_index("sp")
+    t, tx, ty, _ = plane()
+    half = send_ref.shape[1] // 2
+    low, high = pl.ds(0, half), pl.ds(half, half)
+    x_dev, y_dev = (s, tx), (s, ty)
+    greet([(lax.rem(s + k, n), t) for k in range(1, n)] + [x_dev, y_dev])
+    copies = []
+
+    def go(*args):
+        copy = remote(*args)
+        copy.start()
+        copies.append(copy)
+        return copy
+
+    incoming = [None]
+    full = []
+
+    def stage_a(j):
+        source = lax.rem(s - j + n, n)
+        if j:
+            z_copies[j].wait_recv()
+        src = out_ref.at[t, source] if j else send_ref.at[source]
+        full.append(
+            (
+                go(src, out_ref.at[t, source], xs.at[j], xr.at[j], x_dev),
+                go(src, out_ref.at[t, source], ys.at[j], yr.at[j], y_dev),
+            )
+        )
+
+    halves = []
+
+    def stage_b(j):
+        source = lax.rem(s - j + n, n)
+        full[j][0].wait_recv()
+        part = out_ref.at[tx, source, low]
+        halves.append(go(part, part, yhs.at[j], yhr.at[j], y_dev))
+        full[j][1].wait_recv()
+        part = out_ref.at[ty, source, high]
+        halves.append(go(part, part, xhs.at[j], xhr.at[j], x_dev))
+
+    z_copies = [None]
+    for k in range(1, n):
+        target = lax.rem(s + k, n)
+        z_copies.append(
+            go(send_ref.at[target], out_ref.at[t, s], zs.at[k], zr.at[k], (target, t))
+        )
+    stage_a(0)
+    out_ref[t, s] = send_ref[s]
+    for j in range(1, n):
+        stage_a(j)
+        stage_b(j - 1)
+    stage_b(n - 1)
+    for copy in halves:
+        copy.wait_recv()
+    for copy in copies:
+        copy.wait_send()
+
+
+def dispatch(sending):
+    n, capacity, width = sending.shape
+    sem = pltpu.SemaphoreType.DMA((n,))
+    return pl.pallas_call(
+        functools.partial(dispatch_kernel, n),
+        out_shape=jax.ShapeDtypeStruct((4, n, capacity, width), sending.dtype),
+        in_specs=[pl.BlockSpec(memory_space=pltpu.VMEM)],
+        out_specs=pl.BlockSpec(memory_space=pltpu.VMEM),
+        scratch_shapes=[sem] * 10,
+        compiler_params=pltpu.CompilerParams(collective_id=0, has_side_effects=True),
+    )(sending)
+
+
+def return_kernel(
+    n, part_ref, out_ref, bx1, by1, bx2, by2, acc, fin,
+    x1s, x1r, y1s, y1r, x2s, x2r, y2s, y2r, zls, zlr, zhs, zhr,
+):
+    s = lax.axis_index("sp")
+    t, tx, ty, td = plane()
+    half = part_ref.shape[2] // 2
+    low, high = pl.ds(0, half), pl.ds(half, half)
+    x_dev, y_dev = (s, tx), (s, ty)
+    greet([(lax.rem(s + k, n), t) for k in range(1, n)] + [x_dev, y_dev])
+    copies = []
+
+    def go(*args):
+        copy = remote(*args)
+        copy.start()
+        copies.append(copy)
+        return copy
+
+    def total(a, b):
+        return (a.astype(jnp.float32) + b.astype(jnp.float32)).astype(jnp.bfloat16)
+
+    order = list(range(1, n)) + [0]
+    first = []
+    for j in order:
+        owner = lax.rem(s + j, n)
+        first.append(
+            (
+                go(part_ref.at[td, owner, low], bx1.at[j, 1], x1s.at[j, 1], x1r.at[j, 1], x_dev),
+                go(part_ref.at[td, owner, high], by1.at[j, 1], y1s.at[j, 1], y1r.at[j, 1], y_dev),
+                go(part_ref.at[tx, owner, low], bx1.at[j, 0], x1s.at[j, 0], x1r.at[j, 0], x_dev),
+                go(part_ref.at[ty, owner, high], by1.at[j, 0], y1s.at[j, 0], y1r.at[j, 0], y_dev),
+            )
+        )
+    second = []
+    back = []
+
+    def middle(i):
+        j = order[i]
+        owner = lax.rem(s + j, n)
+        first[i][0].wait_recv()
+        acc[j, 0] = total(part_ref[ty, owner, low], bx1[j, 1])
+        to_y = go(acc.at[j, 0], by2.at[j], y2s.at[j], y2r.at[j], y_dev)
+        first[i][1].wait_recv()
+        acc[j, 1] = total(part_ref[tx, owner, high], by1[j, 1])
+        to_x = go(acc.at[j, 1], bx2.at[j], x2s.at[j], x2r.at[j], x_dev)
+        second.append((to_y, to_x))
+
+    def last(i):
+        j = order[i]
+        owner = lax.rem(s + j, n)
+        first[i][2].wait_recv()
+        second[i][0].wait_recv()
+        lower = total(
+            part_ref[t, owner, low].astype(jnp.float32) + bx1[j, 0].astype(jnp.float32), by2[j]
+        )
+        first[i][3].wait_recv()
+        second[i][1].wait_recv()
+        upper = total(
+            part_ref[t, owner, high].astype(jnp.float32) + by1[j, 0].astype(jnp.float32), bx2[j]
+        )
+        if j:
+            fin[j, low] = lower
+            back.append(go(fin.at[j, low], out_ref.at[s, low], zls.at[j], zlr.at[j], (owner, t)))
+            fin[j, high] = upper
+            back.append(go(fin.at[j, high], out_ref.at[s, high], zhs.at[j], zhr.at[j], (owner, t)))
+        else:
+            out_ref[s, low] = lower
+            out_ref[s, high] = upper
+
+    middle(0)
+    for i in range(1, n):
+        middle(i)
+        last(i - 1)
+    last(n - 1)
+    for copy in back:
+        copy.wait_recv()
+    for copy in copies:
+        copy.wait_send()
+
+
+def give_back(partial_value):
+    _, n, capacity, width = partial_value.shape
+    half = capacity // 2
+    kind = partial_value.dtype
+    one = pltpu.SemaphoreType.DMA((n,))
+    two = pltpu.SemaphoreType.DMA((n, 2))
+    return pl.pallas_call(
+        functools.partial(return_kernel, n),
+        out_shape=jax.ShapeDtypeStruct((n, capacity, width), kind),
+        in_specs=[pl.BlockSpec(memory_space=pltpu.VMEM)],
+        out_specs=pl.BlockSpec(memory_space=pltpu.VMEM),
+        scratch_shapes=[
+            pltpu.VMEM((n, 2, half, width), kind),
+            pltpu.VMEM((n, 2, half, width), kind),
+            pltpu.VMEM((n, half, width), kind),
+            pltpu.VMEM((n, half, width), kind),
+            pltpu.VMEM((n, 2, half, width), kind),
+            pltpu.VMEM((n, capacity, width), kind),
+            two, two, two, two, one, one, one, one, one, one, one, one,
+        ],
+        compiler_params=pltpu.CompilerParams(collective_id=1, has_side_effects=True),
+    )(partial_value)
 
 
 def with_halo(block, sides, width):
@@ -118,25 +324,33 @@
         "ts,td->sd", first_place + second_place, normed, preferred_element_type=jnp.float32
     )
     sending = sending.astype(jnp.bfloat16).reshape(sp_count, capacity, width)
-    piece = lax.all_gather(
-        lax.all_to_all(sending, "sp", split_axis=0, concat_axis=0, tiled=True),
-        "tp",
-        axis=0,
-        tiled=True,
-    )
+    in_plane = lax.axis_size("tp") == 4 and capacity % 32 == 0
+    if in_plane:
+        piece = dispatch(sending)
+    else:
+        piece = lax.all_gather(
+            lax.all_to_all(sending, "sp", split_axis=0, concat_axis=0, tiled=True),
+            "tp",
+            axis=0,
+            tiled=True,
+        )
     flat = piece.reshape(-1, piece.shape[-1])
     gate = jnp.dot(flat, gate_weight[0], preferred_element_type=jnp.float32)
     upward = jnp.dot(flat, up_weight[0], preferred_element_type=jnp.float32)
     hidden = (jax.nn.silu(gate) * upward).astype(jnp.bfloat16)
     partial_value = jnp.dot(hidden, down_weight[0], preferred_element_type=jnp.float32)
     partial_value = partial_value.reshape(piece.shape[:-1] + (down_weight.shape[-1],))
-    returned = lax.all_to_all(
-        lax.psum_scatter(partial_value.astype(jnp.bfloat16), "tp", scatter_dimension=0, tiled=True),
-        "sp",
-        split_axis=0,
-        concat_axis=0,
-        tiled=True,
-    )
+    partial_value = partial_value.astype(jnp.bfloat16)
+    if in_plane:
+        returned = give_back(partial_value)
+    else:
+        returned = lax.all_to_all(
+            lax.psum_scatter(partial_value, "tp", scatter_dimension=0, tiled=True),
+            "sp",
+            split_axis=0,
+            concat_axis=0,
+            tiled=True,
+        )
     gathered_back = returned.reshape(slot_total, width)
     first_pick = jnp.dot(first_place, gathered_back, preferred_element_type=jnp.float32)
     second_pick = jnp.dot(second_place, gathered_back, preferred_element_type=jnp.float32)

time: 269 us -> 210 us (0.78)
  waiting for transfers between devices: 165 us -> 35.3 us
  Pallas kernels: 0 us -> 103 us
  blocking collectives: 31.1 us -> 0 us
  starting transfers between devices: 12.6 us -> 7.91 us
    pallas_call x0 -> x2, Pallas kernels: none -> 103 us  [the longest x1 56.2 us: give_back(): pl.pallas_call(functools.partial(return_kernel, n), out_shape=jax.ShapeDt...]
    reduce_scatter x1 -> x0, waiting for transfers between devices: 52.8 us -> none  [local(): lax.psum_scatter(partial_value.astype(jnp.bfloat16), 'tp', scatter_dimens...]
    all_gather x1 -> x0, waiting for transfers between devices: 50.3 us -> none  [local(): lax.all_gather(lax.all_to_all(sending, 'sp', split_axis=0, concat_axis=0,...]
    all_to_all x1 -> x0, blocking collectives: 31.1 us -> none  [local(): lax.all_to_all(sending, 'sp', split_axis=0, concat_axis=0, tiled=True)]
    all_to_all x1 -> x0, waiting for transfers between devices: 26.5 us -> none  [local(): lax.all_to_all(lax.psum_scatter(partial_value.astype(jnp.bfloat16), 'tp',...]
    all_to_all x1 -> x0, starting transfers between devices: 4.6 us -> none  [local(): lax.all_to_all(lax.psum_scatter(partial_value.astype(jnp.bfloat16), 'tp',...]
  transfers between devices with their start and end apart: 7 -> 4, of which waited for: 6 -> 3; matrix products, arithmetic and copies ran while one was open for 1% -> 2% of each run, Pallas kernels for 0% -> 0%
where the time goes in v1:
time: 210 us; the launch traced here: 207 us
  Pallas kernels  103 us (49%)
  waiting for transfers between devices  35.3 us (17%)
  matrix products  34.6 us (16%)
  between operations  13.7 us (7%)
  local copies, waits for them, and re-layouts  8.41 us (4%)
  starting transfers between devices  7.91 us (4%)
  other arithmetic  4.68 us (2%)
    pallas_call x1, Pallas kernels, give_back(): pl.pallas_call(functools.partial(return_kernel, n), out_shape=jax.ShapeDt...  56.2 us
    pallas_call x1, Pallas kernels, dispatch(): pl.pallas_call(functools.partial(dispatch_kernel, n), out_shape=jax.Shape...  46.3 us
    all_gather x1, waiting for transfers between devices, local(): lax.all_gather(attention, 'tp', axis=1, tiled=True)  29 us
    dot_general x1, matrix products, local(): upward = jnp.dot(flat, up_weight[0], preferred_element_type=jnp.float32)  9.04 us
    dot_general x1, matrix products, local(): gate = jnp.dot(flat, gate_weight[0], preferred_element_type=jnp.float32)  8.93 us
    dot_general x1, matrix products, local(): jnp.dot(hidden, down_weight[0], preferred_element_type=jnp.float32)  7.12 us
    all_to_all x1, waiting for transfers between devices, local(): lax.all_to_all(columns.astype(jnp.bfloat16), 'tp', split_axis=0, concat_a...  5.24 us
  transfers between devices with their start and end apart: 4, of which 3 were waited for; matrix products, arithmetic and copies ran while one was open for 2% of the time, Pallas kernels for 0%

profile of v1, /device:TPU:0, one launch (start us, length us, event | category | flops | bytes accessed | tf_op | source)
XLA Modules:
  0.0 207.2 jit_solution(8303862507253325846)
XLA Ops:
  6.5 1.1 constant_dynamic-update-slice_fusion.1
  7.6 0.9 constant_dynamic-update-slice_fusion
  8.5 0.7 fusion.31
  9.2 3.0 %collective-permute-start = (bf16[128,512]{1,0:T(8,128)(2,1)}, bf16[128,512]{1,0:T(8,128)(2,1)}, u32[]{:S(2)}, u32[]{:S(2)}) collective-permute-start(bf16[128,512]{1,0:T(8,128)(2,1)} %get-tuple-element.9), channel_id=1, source_target_pairs={{0,4},{4,8},{8,12},{12,16},{16,20},{20,24},{24,28},{1,5},{5,9},{9,... | collective-permute-start | bytes 393224 | tf_op jit(solution)/shard_map/ppermute | solution.py:227
  12.2 1.3 collective-permute-start.1
  13.9 1.3 reshape.167
  15.1 0.7 max.18
  16.1 1.1 collective-permute-done.1
  17.1 1.7 pad_maximum_fusion.2
  18.9 1.1 copy.34
  20.0 0.8 copy.36
  20.8 1.1 pad_maximum_fusion
  22.0 0.7 fusion.12
  22.8 0.7 fusion.11
  23.5 1.0 fusion.18
  24.5 0.3 copy.40
  24.8 0.7 copy.57
  25.9 0.2 reduce_window_sum.11
  26.0 0.2 select_reduce_fusion
  26.6 29.0 %all-gather.2.cloned.1.call-done = bf16[256,2048]{0,1:T(8,128)(2,1)} async-done(((bf16[256,512]{0,1:T(8,128)(2,1)}), bf16[256,2048]{0,1:T(8,128)(2,1)}) %all-gather.2.cloned.1.call-update) | async-done | bytes 1048592 | tf_op jit(solution)/shard_map/all_gather | solution.py:295
  55.6 2.7 %convolution_convert_fusion.1 = bf16[256,512]{1,0:T(8,128)(2,1)} fusion(bf16[256,2048]{0,1:T(8,128)(2,1)} %all-gather.2.cloned.1.call-done, bf16[2048,512]{1,0:T(8,128)(2,1)S(1)} %copy-done), kind=kOutput, calls=%fused_computation.20 | convolution fusion | flops 537001984 | bytes 3407872 | tf_op jit(solution)/shard_map/dot_general | solution.py:294
  58.2 3.6 %all-to-all-start = ((bf16[4,64,512]{2,1,0:T(8,128)(2,1)}), bf16[4,64,512]{2,1,0:T(8,128)(2,1)S(1)}, u32[]{:S(2)}, u32[]{:S(2)}) async-start(bf16[4,64,512]{2,1,0:T(8,128)(2,1)} %bitcast.11), calls=%async_computation | async-start | bytes 524288 | tf_op jit(solution)/shard_map/all_to_all | solution.py:299
  61.9 5.2 %all-to-all-done = bf16[4,64,512]{2,1,0:T(8,128)(2,1)S(1)} async-done(((bf16[4,64,512]{2,1,0:T(8,128)(2,1)}), bf16[4,64,512]{2,1,0:T(8,128)(2,1)S(1)}, u32[]{:S(2)}, u32[]{:S(2)}) %all-to-all-start) | async-done | bytes 262176 | tf_op jit(solution)/shard_map/all_to_all | solution.py:299
  67.2 0.2 multiply_reduce_fusion
  67.4 1.5 convolution_convert_fusion
  68.9 46.3 %shard_map.118 = bf16[4,8,32,2048]{3,2,1,0:T(8,128)(2,1)} custom-call(bf16[8,32,2048]{2,1,0:T(8,128)(2,1)} %bitcast.90), custom_call_target="tpu_custom_call" | custom-call | tf_op jit(solution)/shard_map/pallas_call | solution.py:108
  115.2 9.0 %fusion.2 = f32[1024,1280]{1,0:T(8,128)S(1)} fusion(bf16[1024,2048]{1,0:T(8,128)(2,1)} %bitcast.88, bf16[1,2048,1280]{2,1,0:T(8,128)(2,1)} %param.22), kind=kOutput, calls=%fused_computation.2 | convolution fusion | flops 5368709120 | bytes 14680064 | tf_op jit(solution)/shard_map/dot_general | solution.py:339
  124.3 8.9 %multiply_convert_fusion = bf16[1024,1280]{1,0:T(8,128)(2,1)S(1)} fusion(f32[1024,1280]{1,0:T(8,128)S(1)} %fusion.2, bf16[1024,2048]{1,0:T(8,128)(2,1)S(1)} %bitcast.89, bf16[1,2048,1280]{2,1,0:T(8,128)(2,1)} %param.21), kind=kOutput, calls=%fused_computation.6 | convolution fusion | flops 5376573440 | bytes 17301504 | tf_op jit(solution)/shard_map/dot_general | solution.py:338
  133.2 7.1 %fusion.8.part_ref = bf16[4,8,32,2048]{3,2,1,0:T(8,128)(2,1)} fusion(bf16[4,8,32,1280]{3,2,1,0:T(8,128)(2,1)S(1)} %bitcast.100, bf16[1,1280,2048]{2,1,0:T(8,128)(2,1)S(1)} %bitcast.99), kind=kOutput, calls=%fused_computation.7 | convolution fusion | flops 5370806272 | bytes 12058624 | tf_op jit(solution)/shard_map/dot_general | solution.py:341
  140.4 56.2 %shard_map.119 = bf16[8,32,2048]{2,1,0:T(8,128)(2,1)} custom-call(bf16[4,8,32,2048]{3,2,1,0:T(8,128)(2,1)} %fusion.8.part_ref), custom_call_target="tpu_custom_call" | custom-call | tf_op jit(solution)/shard_map/pallas_call | solution.py:204
  196.6 1.5 convolution_multiply_fusion.1
  198.1 2.2 %fusion.15 = bf16[64,2048]{1,0:T(8,128)(2,1)} fusion(f32[64,2048]{1,0:T(8,128)S(1)} %convolution_multiply_fusion.1, bf16[256,2048]{1,0:T(8,128)(2,1)} %bitcast.84, f32[64]{0:T(128)S(1)} %get-tuple-element.11, f32[64,2048]{1,0:T(8,128)S(1)} %bitcast.87, bf16[64,2048]{1,0:T(8,128)(2,1)S(1)} %copy-done.2, pred[64,2,256]{2,0,1:T(32,128)(4,1)S(1)} %get-tuple-element.13), kind=kOutput, calls=%fused_computation.18 | convolution fusion | flops 67895296 | bytes 2638336 | tf_op jit(solution)/shard_map/dot_general | solution.py:356
  (40 shorter events, 1.5 us)
Async XLA Ops:
  6.5 49.0 %copy-start = (bf16[2048,512]{1,0:T(8,128)(2,1)S(1)}, bf16[2048,512]{1,0:T(8,128)(2,1)}, u32[]{:S(2)}) copy-start(bf16[2048,512]{1,0:T(8,128)(2,1)} %param.16) | copy-start | bytes 6291460
  6.5 49.0 %all-gather.2.cloned.1.call-start = ((), (), s32[]{:S(2)}) async-start(), calls=%async_computation.1 | async-start | bytes 1310720 | tf_op jit(solution)/shard_map/all_gather | solution.py:295
  9.2 6.9 %collective-permute-start = (bf16[128,512]{1,0:T(8,128)(2,1)}, bf16[128,512]{1,0:T(8,128)(2,1)}, u32[]{:S(2)}, u32[]{:S(2)}) collective-permute-start(bf16[128,512]{1,0:T(8,128)(2,1)} %get-tuple-element.9), channel_id=1, source_target_pairs={{0,4},{4,8},{8,12},{12,16},{16,20},{20,24},{24,28},{1,5},{5,9},{9,... | collective-permute-start | bytes 393224 | tf_op jit(solution)/shard_map/ppermute | solution.py:227
  12.2 4.9 %collective-permute-start.1 = (bf16[128,512]{1,0:T(8,128)(2,1)S(1)}, bf16[128,512]{1,0:T(8,128)(2,1)}, u32[]{:S(2)}, u32[]{:S(2)}) collective-permute-start(bf16[128,512]{1,0:T(8,128)(2,1)S(1)} %get-tuple-element.10), channel_id=1, source_target_pairs={{4,0},{8,4},{12,8},{16,12},{20,16},{24,20},{28,24},{5,1},{9,5},{13... | collective-permute-start | bytes 393224 | tf_op jit(solution)/shard_map/ppermute | solution.py:230
  23.5 2.0 copy-start.4
  24.5 37.4 %copy-start.5 = (f32[64,2]{0,1:T(2,128)S(1)}, f32[64,2]{0,1:T(2,128)}, u32[]{:S(2)}) copy-start(f32[64,2]{0,1:T(2,128)} %param.20) | copy-start | bytes 1540
  26.6 40.6 %copy-start.2 = (bf16[64,2048]{1,0:T(8,128)(2,1)S(1)}, bf16[64,2048]{1,0:T(8,128)(2,1)}, u32[]{:S(2)}) copy-start(bf16[64,2048]{1,0:T(8,128)(2,1)} %param.17) | copy-start | bytes 786436
  26.6 40.8 %copy-start.3 = (f32[2048]{0:T(1024)S(1)}, f32[2048]{0:T(1024)}, u32[]{:S(2)}) copy-start(f32[2048]{0:T(1024)} %param.18) | copy-start | bytes 24580
  58.2 8.9 %all-to-all-start = ((bf16[4,64,512]{2,1,0:T(8,128)(2,1)}), bf16[4,64,512]{2,1,0:T(8,128)(2,1)S(1)}, u32[]{:S(2)}, u32[]{:S(2)}) async-start(bf16[4,64,512]{2,1,0:T(8,128)(2,1)} %bitcast.11), calls=%async_computation | async-start | bytes 524288 | tf_op jit(solution)/shard_map/all_to_all | solution.py:299
  115.2 9.1 %copy-start.1 = (bf16[4,8,32,2048]{3,2,1,0:T(8,128)(2,1)S(1)}, bf16[4,8,32,2048]{3,2,1,0:T(8,128)(2,1)}, u32[]{:S(2)}) copy-start(bf16[4,8,32,2048]{3,2,1,0:T(8,128)(2,1)} %shard_map.118) | copy-start | bytes 12582916
  115.2 18.0 %slice-start = ((s8[5242880]{0:T(1024)(128)(4,1)}), s8[4194304]{0:T(1024)(128)(4,1)S(1)}, s32[]{:S(2)}) async-start(s8[5242880]{0:T(1024)(128)(4,1)} %bitcast.98), calls=%async_computation.2 | async-start | bytes 8388608
  124.3 9.0 %slice-start.1 = ((s8[5242880]{0:T(1024)(128)(4,1)}), s8[1048576]{0:T(1024)(128)(4,1)S(1)}, s32[]{:S(2)}) async-start(s8[5242880]{0:T(1024)(128)(4,1)} %bitcast.98), calls=%async_computation.3 | async-start | bytes 2097152
Sparse Core Ops, SparseCore 0:
  25.6 29.8 all-gather.1

commit v2 on v1

--- a/solution.py
+++ b/solution.py
@@ -138,7 +138,9 @@
 
     order = list(range(1, n)) + [0]
     first = []
-    for j in order:
+
+    def begin(i):
+        j = order[i]
         owner = lax.rem(s + j, n)
         first.append(
             (
@@ -148,6 +150,7 @@
                 go(part_ref.at[ty, owner, high], by1.at[j, 0], y1s.at[j, 0], y1r.at[j, 0], y_dev),
             )
         )
+
     second = []
     back = []
 
@@ -184,8 +187,12 @@
             out_ref[s, low] = lower
             out_ref[s, high] = upper
 
+    begin(0)
+    begin(1)
     middle(0)
     for i in range(1, n):
+        if i + 1 < n:
+            begin(i + 1)
         middle(i)
         last(i - 1)
     last(n - 1)
@@ -219,6 +226,89 @@
     )(partial_value)
 
 
+def project_kernel(x_ref, w_ref, out_ref, buf, acc, cols, gs, gr, as_, ar):
+    s = lax.axis_index("sp")
+    t, tx, ty, td = plane()
+    rows, depth = x_ref.shape
+    half = rows // 2
+    low, high = pl.ds(0, half), pl.ds(half, half)
+    x_dev, y_dev, d_dev = (s, tx), (s, ty), (s, td)
+    greet([x_dev, y_dev, d_dev])
+    copies = []
+
+    def go(*args):
+        copy = remote(*args)
+        copy.start()
+        copies.append(copy)
+        return copy
+
+    def product(piece, owner, columns):
+        weight = w_ref[pl.ds(pl.multiple_of(owner * depth, depth), depth), columns]
+        return jnp.dot(piece, weight, preferred_element_type=jnp.float32)
+
+    x_low = go(x_ref.at[low], buf.at[t, low], gs.at[0], gr.at[0], x_dev)
+    y_high = go(x_ref.at[high], buf.at[t, high], gs.at[1], gr.at[1], y_dev)
+    x_high = go(x_ref.at[high], buf.at[t, high], gs.at[2], gr.at[2], x_dev)
+    y_low = go(x_ref.at[low], buf.at[t, low], gs.at[3], gr.at[3], y_dev)
+    acc[...] = product(x_ref[...], t, slice(None))
+    x_low.wait_recv()
+    d_low = go(buf.at[tx, low], buf.at[tx, low], gs.at[4], gr.at[4], y_dev)
+    y_high.wait_recv()
+    d_high = go(buf.at[ty, high], buf.at[ty, high], gs.at[5], gr.at[5], x_dev)
+    x_high.wait_recv()
+    acc[...] += product(buf[tx], tx, slice(None))
+    y_low.wait_recv()
+    acc[...] += product(buf[ty], ty, slice(None))
+    d_low.wait_recv()
+    d_high.wait_recv()
+    tiles = 2
+    width = w_ref.shape[1] // tiles
+    own = rows // 4
+    arrivals = []
+    for tile in range(tiles):
+        columns = slice(tile * width, (tile + 1) * width)
+        total = acc[:, columns] + product(buf[td], td, columns)
+        cols[tile] = total.astype(cols.dtype)
+        for k, (owner, device) in enumerate(((td, d_dev), (tx, x_dev), (ty, y_dev))):
+            arrivals.append(
+                go(
+                    cols.at[tile, pl.ds(pl.multiple_of(owner * own, own), own)],
+                    out_ref.at[tile, t],
+                    as_.at[tile, k],
+                    ar.at[tile, k],
+                    device,
+                )
+            )
+        out_ref[tile, t] = cols[tile, pl.ds(pl.multiple_of(t * own, own), own)]
+    for copy in arrivals:
+        copy.wait_recv()
+    for copy in copies:
+        copy.wait_send()
+
+
+def project(attention, out_weight):
+    rows, depth = attention.shape
+    width = out_weight.shape[1]
+    kind = attention.dtype
+    out = pl.pallas_call(
+        project_kernel,
+        out_shape=jax.ShapeDtypeStruct((2, 4, rows // 4, width // 2), kind),
+        in_specs=[pl.BlockSpec(memory_space=pltpu.VMEM)] * 2,
+        out_specs=pl.BlockSpec(memory_space=pltpu.VMEM),
+        scratch_shapes=[
+            pltpu.VMEM((4, rows, depth), kind),
+            pltpu.VMEM((rows, width), jnp.float32),
+            pltpu.VMEM((2, rows, width // 2), kind),
+            pltpu.SemaphoreType.DMA((6,)),
+            pltpu.SemaphoreType.DMA((6,)),
+            pltpu.SemaphoreType.DMA((2, 3)),
+            pltpu.SemaphoreType.DMA((2, 3)),
+        ],
+        compiler_params=pltpu.CompilerParams(collective_id=2, has_side_effects=True),
+    )(attention, out_weight)
+    return out.transpose(2, 1, 0, 3).reshape(rows // 4, 4 * width)
+
+
 def with_halo(block, sides, width):
     for axis, dim in sides:
         count = lax.axis_size(axis)
@@ -291,21 +381,25 @@
     down_weight,
 ):
     attention = attend_local(queries, keys, values, sink_logit)
-    columns = jnp.dot(
-        lax.all_gather(attention, "tp", axis=1, tiled=True),
-        out_weight,
-        preferred_element_type=jnp.float32,
-    )
-    projected = lax.all_to_all(
-        columns.astype(jnp.bfloat16), "tp", split_axis=0, concat_axis=1, tiled=True
-    )
+    capacity = max(2, 4 * residual.shape[0] // lax.axis_size("sp"))
+    in_plane = lax.axis_size("tp") == 4 and capacity % 32 == 0
+    if in_plane:
+        projected = project(attention, out_weight)
+    else:
+        columns = jnp.dot(
+            lax.all_gather(attention, "tp", axis=1, tiled=True),
+            out_weight,
+            preferred_element_type=jnp.float32,
+        )
+        projected = lax.all_to_all(
+            columns.astype(jnp.bfloat16), "tp", split_axis=0, concat_axis=1, tiled=True
+        )
     hidden_state = residual.astype(jnp.float32) + projected.astype(jnp.float32)
     inverse = lax.rsqrt(jnp.mean(hidden_state * hidden_state, axis=-1, keepdims=True) + EPS)
     normed = (hidden_state * inverse * norm_gain).astype(jnp.bfloat16)
     sp_count = lax.axis_size("sp")
     tok_rows = residual.shape[0]
     width = residual.shape[1]
-    capacity = max(2, 4 * tok_rows // sp_count)
     slot_total = sp_count * capacity
     expert_ids = routes.reshape(-1)
     onehot = (expert_ids[:, None] == jnp.arange(sp_count, dtype=jnp.int32)[None, :]).astype(
@@ -324,7 +418,6 @@
         "ts,td->sd", first_place + second_place, normed, preferred_element_type=jnp.float32
     )
     sending = sending.astype(jnp.bfloat16).reshape(sp_count, capacity, width)
-    in_plane = lax.axis_size("tp") == 4 and capacity % 32 == 0
     if in_plane:
         piece = dispatch(sending)
     else:

time: 210 us -> 168 us (0.80); the launches traced: 207 us -> 167 us
  waiting for transfers between devices: 35.3 us -> 0.01 us
  Pallas kernels: 103 us -> 119 us
  between operations: 13.7 us -> 0.32 us
  starting transfers between devices: 7.91 us -> 3.7 us
  matrix products: 34.6 us -> 32 us
    all_gather x1 -> x0, waiting for transfers between devices: 29 us -> none  [local(): lax.all_gather(attention, 'tp', axis=1, tiled=True)]
    pallas_call x0 -> x1, Pallas kernels: none -> 20.4 us  [project(): pl.pallas_call(project_kernel, out_shape=jax.ShapeDtypeStruct((2, 4, rows...]
    pallas_call x1, Pallas kernels: 56.2 us -> 49.2 us  [give_back(): pl.pallas_call(functools.partial(return_kernel, n), out_shape=jax.ShapeDt...]
    all_to_all x1 -> x0, waiting for transfers between devices: 5.24 us -> none  [local(): lax.all_to_all(columns.astype(jnp.bfloat16), 'tp', split_axis=0, concat_a...]
    all_to_all x1 -> x0, starting transfers between devices: 3.59 us -> none  [local(): lax.all_to_all(columns.astype(jnp.bfloat16), 'tp', split_axis=0, concat_a...]
    pallas_call x1, Pallas kernels: 46.3 us -> 49.3 us  [dispatch(): pl.pallas_call(functools.partial(dispatch_kernel, n), out_shape=jax.Shape...]
    dot_general x1 -> x0, matrix products: 2.65 us -> none  [local(): jnp.dot(lax.all_gather(attention, 'tp', axis=1, tiled=True), out_weight,...]
  transfers between devices with their start and end apart: 4 -> 2, of which waited for: 3 -> 0; matrix products, arithmetic and copies ran while one was open for 2% -> 3% of each run, Pallas kernels for 0% -> 0%
where the time goes in v2:
time: 168 us; the launch traced here: 167 us
  Pallas kernels  119 us (71%)
  matrix products  32 us (19%)
  local copies, waits for them, and re-layouts  8.79 us (5%)
  other arithmetic  3.71 us (2%)
  starting transfers between devices  3.7 us (2%)
    pallas_call x1, Pallas kernels, dispatch(): pl.pallas_call(functools.partial(dispatch_kernel, n), out_shape=jax.Shape...  49.3 us
    pallas_call x1, Pallas kernels, give_back(): pl.pallas_call(functools.partial(return_kernel, n), out_shape=jax.ShapeDt...  49.2 us
    pallas_call x1, Pallas kernels, project(): pl.pallas_call(project_kernel, out_shape=jax.ShapeDtypeStruct((2, 4, rows...  20.4 us
    dot_general x1, matrix products, local(): upward = jnp.dot(flat, up_weight[0], preferred_element_type=jnp.float32)  9.04 us
    dot_general x1, matrix products, local(): gate = jnp.dot(flat, gate_weight[0], preferred_element_type=jnp.float32)  8.92 us
    dot_general x1, matrix products, local(): jnp.dot(hidden, down_weight[0], preferred_element_type=jnp.float32)  7.11 us
  transfers between devices with their start and end apart: 2, of which 0 were waited for; matrix products, arithmetic and copies ran while one was open for 3% of the time, Pallas kernels for 0%

profile of v2, /device:TPU:0, one launch (start us, length us, event | category | flops | bytes accessed | tf_op | source)
XLA Modules:
  0.0 167.4 jit_solution(7178913235472032456)
XLA Ops:
  0.0 0.9 constant_dynamic-update-slice_fusion.1
  0.9 0.9 constant_dynamic-update-slice_fusion
  1.9 2.4 %collective-permute-start = (bf16[128,512]{1,0:T(8,128)(2,1)S(1)}, bf16[128,512]{1,0:T(8,128)(2,1)S(1)}, u32[]{:S(2)}, u32[]{:S(2)}) collective-permute-start(bf16[128,512]{1,0:T(8,128)(2,1)S(1)} %get-tuple-element.9), channel_id=1, source_target_pairs={{0,4},{4,8},{8,12},{12,16},{16,20},{20,24},{24,28},{1,5},{5,9},{9,... | collective-permute-start | bytes 393224 | tf_op jit(solution)/shard_map/ppermute | solution.py:317
  4.3 1.3 collective-permute-start.1
  5.6 0.2 copy.36
  5.9 1.3 reshape.165
  7.2 0.7 max.18
  7.9 0.8 copy.44
  8.9 0.2 reduce_window_sum.11
  9.1 0.2 select_reduce_fusion
  9.5 0.7 multiply_add_fusion
  10.3 0.2 broadcast_and_fusion
  10.5 0.8 slice_bitcast_fusion.4
  11.5 0.2 copy.37
  11.9 0.7 fusion.12
  12.7 0.7 fusion.11
  13.4 1.0 fusion.18
  14.4 0.6 copy.52
  15.0 1.0 reshape.166.x_ref
  16.0 20.4 %shard_map.118 = bf16[2,4,64,256]{3,2,1,0:T(8,128)(2,1)} custom-call(bf16[256,512]{1,0:T(8,128)(2,1)} %reshape.166.x_ref, bf16[2048,512]{1,0:T(8,128)(2,1)} %w_ref.1), custom_call_target="tpu_custom_call" | custom-call | tf_op jit(solution)/shard_map/pallas_call | solution.py:293
  36.4 1.0 convert_bitcast_fusion
  37.4 0.4 copy.43
  37.8 0.4 reshape.161
  38.2 0.2 multiply_reduce_fusion
  38.4 1.5 convolution_convert_fusion
  39.9 49.3 %shard_map.119 = bf16[4,8,32,2048]{3,2,1,0:T(8,128)(2,1)} custom-call(bf16[8,32,2048]{2,1,0:T(8,128)(2,1)} %bitcast.75), custom_call_target="tpu_custom_call" | custom-call | tf_op jit(solution)/shard_map/pallas_call | solution.py:108
  89.2 9.0 %fusion.2 = f32[1024,1280]{1,0:T(8,128)S(1)} fusion(bf16[1024,2048]{1,0:T(8,128)(2,1)} %bitcast.73, bf16[1,2048,1280]{2,1,0:T(8,128)(2,1)} %param.22), kind=kOutput, calls=%fused_computation.2 | convolution fusion | flops 5368709120 | bytes 14680064 | tf_op jit(solution)/shard_map/dot_general | solution.py:432
  98.3 8.9 %multiply_convert_fusion = bf16[1024,1280]{1,0:T(8,128)(2,1)S(1)} fusion(f32[1024,1280]{1,0:T(8,128)S(1)} %fusion.2, bf16[1024,2048]{1,0:T(8,128)(2,1)S(1)} %bitcast.74, bf16[1,2048,1280]{2,1,0:T(8,128)(2,1)} %param.21), kind=kOutput, calls=%fused_computation.6 | convolution fusion | flops 5376573440 | bytes 17301504 | tf_op jit(solution)/shard_map/dot_general | solution.py:431
  107.3 7.1 %fusion.8.part_ref = bf16[4,8,32,2048]{3,2,1,0:T(8,128)(2,1)} fusion(bf16[4,8,32,1280]{3,2,1,0:T(8,128)(2,1)S(1)} %bitcast.83, bf16[1,1280,2048]{2,1,0:T(8,128)(2,1)S(1)} %bitcast.82), kind=kOutput, calls=%fused_computation.7 | convolution fusion | flops 5370806272 | bytes 12058624 | tf_op jit(solution)/shard_map/dot_general | solution.py:434
  114.4 49.2 %shard_map.120 = bf16[8,32,2048]{2,1,0:T(8,128)(2,1)} custom-call(bf16[4,8,32,2048]{3,2,1,0:T(8,128)(2,1)} %fusion.8.part_ref), custom_call_target="tpu_custom_call" | custom-call | tf_op jit(solution)/shard_map/pallas_call | solution.py:211
  163.6 1.5 convolution_multiply_fusion.1
  165.1 2.2 %fusion.15 = bf16[64,2048]{1,0:T(8,128)(2,1)} fusion(f32[64,2048]{1,0:T(8,128)S(1)} %convolution_multiply_fusion.1, bf16[256,2048]{1,0:T(8,128)(2,1)} %bitcast.72, f32[64]{0:T(128)S(1)} %get-tuple-element.11, f32[64,2048]{1,0:T(8,128)S(1)} %reshape.161, bf16[64,2048]{1,0:T(8,128)(2,1)S(1)} %copy-done.1, pred[64,2,256]{2,0,1:T(32,128)(4,1)S(1)} %get-tuple-element.13), kind=kOutput, calls=%fused_computation.18 | convolution fusion | flops 67895296 | bytes 2638336 | tf_op jit(solution)/shard_map/dot_general | solution.py:449
  (30 shorter events, 1.3 us)
Async XLA Ops:
  1.9 9.4 %collective-permute-start = (bf16[128,512]{1,0:T(8,128)(2,1)S(1)}, bf16[128,512]{1,0:T(8,128)(2,1)S(1)}, u32[]{:S(2)}, u32[]{:S(2)}) collective-permute-start(bf16[128,512]{1,0:T(8,128)(2,1)S(1)} %get-tuple-element.9), channel_id=1, source_target_pairs={{0,4},{4,8},{8,12},{12,16},{16,20},{20,24},{24,28},{1,5},{5,9},{9,... | collective-permute-start | bytes 393224 | tf_op jit(solution)/shard_map/ppermute | solution.py:317
  4.3 7.0 %collective-permute-start.1 = (bf16[128,512]{1,0:T(8,128)(2,1)S(1)}, bf16[128,512]{1,0:T(8,128)(2,1)S(1)}, u32[]{:S(2)}, u32[]{:S(2)}) collective-permute-start(bf16[128,512]{1,0:T(8,128)(2,1)S(1)} %get-tuple-element.10), channel_id=1, source_target_pairs={{4,0},{8,4},{12,8},{16,12},{20,16},{24,20},{28,24},{5,1},{9,5},{13... | collective-permute-start | bytes 393224 | tf_op jit(solution)/shard_map/ppermute | solution.py:320
  15.0 23.2 %copy-start.1 = (bf16[64,2048]{1,0:T(8,128)(2,1)S(1)}, bf16[64,2048]{1,0:T(8,128)(2,1)}, u32[]{:S(2)}) copy-start(bf16[64,2048]{1,0:T(8,128)(2,1)} %param.17) | copy-start | bytes 786436
  16.0 22.4 %copy-start.2 = (f32[2048]{0:T(1024)S(1)}, f32[2048]{0:T(1024)}, u32[]{:S(2)}) copy-start(f32[2048]{0:T(1024)} %param.18) | copy-start | bytes 24580
  89.2 9.1 %copy-start = (bf16[4,8,32,2048]{3,2,1,0:T(8,128)(2,1)S(1)}, bf16[4,8,32,2048]{3,2,1,0:T(8,128)(2,1)}, u32[]{:S(2)}) copy-start(bf16[4,8,32,2048]{3,2,1,0:T(8,128)(2,1)} %shard_map.119) | copy-start | bytes 12582916
  89.2 18.0 %slice-start = ((s8[5242880]{0:T(1024)(128)(4,1)}), s8[4194304]{0:T(1024)(128)(4,1)S(1)}, s32[]{:S(2)}) async-start(s8[5242880]{0:T(1024)(128)(4,1)} %bitcast.81), calls=%async_computation | async-start | bytes 8388608
  98.3 8.9 %slice-start.1 = ((s8[5242880]{0:T(1024)(128)(4,1)}), s8[1048576]{0:T(1024)(128)(4,1)S(1)}, s32[]{:S(2)}) async-start(s8[5242880]{0:T(1024)(128)(4,1)} %bitcast.81), calls=%async_computation.1 | async-start | bytes 2097152

commit v3 on v2

--- a/solution.py
+++ b/solution.py
@@ -43,13 +43,35 @@
     )
 
 
-def dispatch_kernel(n, send_ref, out_ref, zs, zr, xs, xr, ys, yr, xhs, xhr, yhs, yhr):
+def flipped(index, mask):
+    result = index
+    bit = 1
+    while bit <= mask:
+        if mask & bit:
+            result = result + bit * (1 - 2 * lax.rem(index // bit, 2))
+        bit *= 2
+    return result
+
+
+def expert_kernel(
+    send_ref, gate_hbm, up_hbm, down_hbm, out_ref,
+    gate, up, down, piece, hidden, part, bx1, by1, bx2, by2, acc, fin, load,
+    zs, zr, xs, xr, ys, yr, xhs, xhr, yhs, yhr,
+    x1s, x1r, y1s, y1r, x2s, x2r, y2s, y2r, zls, zlr, zhs, zhr,
+):
+    n, capacity, width = send_ref.shape
     s = lax.axis_index("sp")
-    t, tx, ty, _ = plane()
-    half = send_ref.shape[1] // 2
+    t, tx, ty, td = plane()
+    half = capacity // 2
     low, high = pl.ds(0, half), pl.ds(half, half)
     x_dev, y_dev = (s, tx), (s, ty)
-    greet([(lax.rem(s + k, n), t) for k in range(1, n)] + [x_dev, y_dev])
+    loads = [
+        pltpu.make_async_copy(source, target, load.at[k])
+        for k, (source, target) in enumerate(((gate_hbm, gate), (up_hbm, up), (down_hbm, down)))
+    ]
+    for copy in loads:
+        copy.start()
+    greet([(flipped(s, m), t) for m in range(1, n)] + [x_dev, y_dev])
     copies = []
 
     def go(*args):
@@ -58,172 +80,171 @@
         copies.append(copy)
         return copy
 
-    incoming = [None]
-    full = []
-
-    def stage_a(j):
-        source = lax.rem(s - j + n, n)
-        if j:
-            z_copies[j].wait_recv()
-        src = out_ref.at[t, source] if j else send_ref.at[source]
-        full.append(
-            (
-                go(src, out_ref.at[t, source], xs.at[j], xr.at[j], x_dev),
-                go(src, out_ref.at[t, source], ys.at[j], yr.at[j], y_dev),
-            )
-        )
-
-    halves = []
-
-    def stage_b(j):
-        source = lax.rem(s - j + n, n)
-        full[j][0].wait_recv()
-        part = out_ref.at[tx, source, low]
-        halves.append(go(part, part, yhs.at[j], yhr.at[j], y_dev))
-        full[j][1].wait_recv()
-        part = out_ref.at[ty, source, high]
-        halves.append(go(part, part, xhs.at[j], xhr.at[j], x_dev))
-
-    z_copies = [None]
-    for k in range(1, n):
-        target = lax.rem(s + k, n)
-        z_copies.append(
-            go(send_ref.at[target], out_ref.at[t, s], zs.at[k], zr.at[k], (target, t))
-        )
-    stage_a(0)
-    out_ref[t, s] = send_ref[s]
-    for j in range(1, n):
-        stage_a(j)
-        stage_b(j - 1)
-    stage_b(n - 1)
-    for copy in halves:
-        copy.wait_recv()
-    for copy in copies:
-        copy.wait_send()
-
-
-def dispatch(sending):
-    n, capacity, width = sending.shape
-    sem = pltpu.SemaphoreType.DMA((n,))
-    return pl.pallas_call(
-        functools.partial(dispatch_kernel, n),
-        out_shape=jax.ShapeDtypeStruct((4, n, capacity, width), sending.dtype),
-        in_specs=[pl.BlockSpec(memory_space=pltpu.VMEM)],
-        out_specs=pl.BlockSpec(memory_space=pltpu.VMEM),
-        scratch_shapes=[sem] * 10,
-        compiler_params=pltpu.CompilerParams(collective_id=0, has_side_effects=True),
-    )(sending)
-
-
-def return_kernel(
-    n, part_ref, out_ref, bx1, by1, bx2, by2, acc, fin,
-    x1s, x1r, y1s, y1r, x2s, x2r, y2s, y2r, zls, zlr, zhs, zhr,
-):
-    s = lax.axis_index("sp")
-    t, tx, ty, td = plane()
-    half = part_ref.shape[2] // 2
-    low, high = pl.ds(0, half), pl.ds(half, half)
-    x_dev, y_dev = (s, tx), (s, ty)
-    greet([(lax.rem(s + k, n), t) for k in range(1, n)] + [x_dev, y_dev])
-    copies = []
-
-    def go(*args):
-        copy = remote(*args)
-        copy.start()
-        copies.append(copy)
-        return copy
-
     def total(a, b):
         return (a.astype(jnp.float32) + b.astype(jnp.float32)).astype(jnp.bfloat16)
 
-    order = list(range(1, n)) + [0]
-    first = []
-
-    def begin(i):
-        j = order[i]
-        owner = lax.rem(s + j, n)
-        first.append(
-            (
-                go(part_ref.at[td, owner, low], bx1.at[j, 1], x1s.at[j, 1], x1r.at[j, 1], x_dev),
-                go(part_ref.at[td, owner, high], by1.at[j, 1], y1s.at[j, 1], y1r.at[j, 1], y_dev),
-                go(part_ref.at[tx, owner, low], bx1.at[j, 0], x1s.at[j, 0], x1r.at[j, 0], x_dev),
-                go(part_ref.at[ty, owner, high], by1.at[j, 0], y1s.at[j, 0], y1r.at[j, 0], y_dev),
-            )
-        )
-
-    second = []
-    back = []
-
-    def middle(i):
-        j = order[i]
-        owner = lax.rem(s + j, n)
-        first[i][0].wait_recv()
-        acc[j, 0] = total(part_ref[ty, owner, low], bx1[j, 1])
-        to_y = go(acc.at[j, 0], by2.at[j], y2s.at[j], y2r.at[j], y_dev)
-        first[i][1].wait_recv()
-        acc[j, 1] = total(part_ref[tx, owner, high], by1[j, 1])
-        to_x = go(acc.at[j, 1], bx2.at[j], x2s.at[j], x2r.at[j], x_dev)
-        second.append((to_y, to_x))
-
-    def last(i):
-        j = order[i]
-        owner = lax.rem(s + j, n)
-        first[i][2].wait_recv()
-        second[i][0].wait_recv()
-        lower = total(
-            part_ref[t, owner, low].astype(jnp.float32) + bx1[j, 0].astype(jnp.float32), by2[j]
-        )
-        first[i][3].wait_recv()
-        second[i][1].wait_recv()
-        upper = total(
-            part_ref[t, owner, high].astype(jnp.float32) + by1[j, 0].astype(jnp.float32), bx2[j]
-        )
-        if j:
-            fin[j, low] = lower
-            back.append(go(fin.at[j, low], out_ref.at[s, low], zls.at[j], zlr.at[j], (owner, t)))
-            fin[j, high] = upper
-            back.append(go(fin.at[j, high], out_ref.at[s, high], zhs.at[j], zhr.at[j], (owner, t)))
-        else:
-            out_ref[s, low] = lower
-            out_ref[s, high] = upper
-
-    begin(0)
-    begin(1)
-    middle(0)
-    for i in range(1, n):
-        if i + 1 < n:
-            begin(i + 1)
-        middle(i)
-        last(i - 1)
-    last(n - 1)
+    gray = [k ^ (k >> 1) for k in range(n // 2)]
+    z_copies, full, halves, first, second, back = {}, {}, {}, {}, {}, []
+
+    def members(q):
+        return (2 * q, 2 * q + 1)
+
+    def stage_a(q):
+        for m in members(q):
+            source = flipped(s, m)
+            if m:
+                z_copies[m].wait_recv()
+            src = piece.at[t, source] if m else send_ref.at[source]
+            full[m] = (
+                go(src, piece.at[t, source], xs.at[m], xr.at[m], x_dev),
+                go(src, piece.at[t, source], ys.at[m], yr.at[m], y_dev),
+            )
+
+    def stage_b(q):
+        for m in members(q):
+            source = flipped(s, m)
+            full[m][0].wait_recv()
+            block = piece.at[tx, source, low]
+            to_y = go(block, block, yhs.at[m], yhr.at[m], y_dev)
+            full[m][1].wait_recv()
+            block = piece.at[ty, source, high]
+            halves[m] = (to_y, go(block, block, xhs.at[m], xhr.at[m], x_dev))
+
+    def compute(q):
+        for m in members(q):
+            for copy in halves[m]:
+                copy.wait_recv()
+        base = flipped(s // 2, q) * 2
+        rows = 8 * capacity
+        step = 256
+
+        @pl.loop(0, gate.shape[1] // step)
+        def _(k):
+            columns = pl.ds(pl.multiple_of(k * step, step), step)
+            x = piece[:, pl.ds(base, 2)].reshape(rows, width)
+            g = jnp.dot(x, gate[:, columns], preferred_element_type=jnp.float32)
+            u = jnp.dot(x, up[:, columns], preferred_element_type=jnp.float32)
+            hidden[:, columns] = (jax.nn.silu(g) * u).astype(hidden.dtype)
+
+        wide = 512
+
+        @pl.loop(0, width // wide)
+        def _(k):
+            columns = pl.ds(pl.multiple_of(k * wide, wide), wide)
+            share = jnp.dot(hidden[...], down[:, columns], preferred_element_type=jnp.float32)
+            part[:, pl.ds(base, 2), :, columns] = share.astype(part.dtype).reshape(
+                4, 2, capacity, wide
+            )
+
+    def begin(q):
+        for m in members(q):
+            owner = flipped(s, m)
+            first[m] = (
+                go(part.at[td, owner, low], bx1.at[m, 1], x1s.at[m, 1], x1r.at[m, 1], x_dev),
+                go(part.at[td, owner, high], by1.at[m, 1], y1s.at[m, 1], y1r.at[m, 1], y_dev),
+                go(part.at[tx, owner, low], bx1.at[m, 0], x1s.at[m, 0], x1r.at[m, 0], x_dev),
+                go(part.at[ty, owner, high], by1.at[m, 0], y1s.at[m, 0], y1r.at[m, 0], y_dev),
+            )
+
+    def middle(q):
+        for m in members(q):
+            owner = flipped(s, m)
+            first[m][0].wait_recv()
+            acc[m, 0] = total(part[ty, owner, low], bx1[m, 1])
+            to_y = go(acc.at[m, 0], by2.at[m], y2s.at[m], y2r.at[m], y_dev)
+            first[m][1].wait_recv()
+            acc[m, 1] = total(part[tx, owner, high], by1[m, 1])
+            second[m] = (to_y, go(acc.at[m, 1], bx2.at[m], x2s.at[m], x2r.at[m], x_dev))
+
+    def last(q):
+        for m in members(q):
+            owner = flipped(s, m)
+            first[m][2].wait_recv()
+            second[m][0].wait_recv()
+            lower = total(
+                part[t, owner, low].astype(jnp.float32) + bx1[m, 0].astype(jnp.float32), by2[m]
+            )
+            first[m][3].wait_recv()
+            second[m][1].wait_recv()
+            upper = total(
+                part[t, owner, high].astype(jnp.float32) + by1[m, 0].astype(jnp.float32), bx2[m]
+            )
+            if m:
+                away = (owner, t)
+                fin[m, low] = lower
+                back.append(go(fin.at[m, low], out_ref.at[s, low], zls.at[m], zlr.at[m], away))
+                fin[m, high] = upper
+                back.append(go(fin.at[m, high], out_ref.at[s, high], zhs.at[m], zhr.at[m], away))
+            else:
+                out_ref[s, low] = lower
+                out_ref[s, high] = upper
+
+    for q in gray:
+        for m in members(q):
+            if m:
+                target = flipped(s, m)
+                z_copies[m] = go(
+                    send_ref.at[target], piece.at[t, s], zs.at[m], zr.at[m], (target, t)
+                )
+    stage_a(0)
+    piece[t, s] = send_ref[s]
+    order = gray[1:] + [0]
+    count = len(gray)
+    for k in range(count + 4):
+        if k + 1 < count:
+            stage_a(gray[k + 1])
+        if k < count:
+            stage_b(gray[k])
+        if k == 2:
+            for copy in loads:
+                copy.wait()
+        if 0 <= k - 2 < count:
+            compute(order[k - 2])
+            begin(order[k - 2])
+        if 0 <= k - 3 < count:
+            middle(order[k - 3])
+        if 0 <= k - 4 < count:
+            last(order[k - 4])
     for copy in back:
         copy.wait_recv()
     for copy in copies:
         copy.wait_send()
 
 
-def give_back(partial_value):
-    _, n, capacity, width = partial_value.shape
+def experts(sending, gate_weight, up_weight, down_weight):
+    n, capacity, width = sending.shape
     half = capacity // 2
-    kind = partial_value.dtype
+    kind = sending.dtype
     one = pltpu.SemaphoreType.DMA((n,))
     two = pltpu.SemaphoreType.DMA((n, 2))
+    anywhere = pl.BlockSpec(memory_space=pl.ANY)
     return pl.pallas_call(
-        functools.partial(return_kernel, n),
+        expert_kernel,
         out_shape=jax.ShapeDtypeStruct((n, capacity, width), kind),
-        in_specs=[pl.BlockSpec(memory_space=pltpu.VMEM)],
+        in_specs=[pl.BlockSpec(memory_space=pltpu.VMEM), anywhere, anywhere, anywhere],
         out_specs=pl.BlockSpec(memory_space=pltpu.VMEM),
         scratch_shapes=[
+            pltpu.VMEM(gate_weight.shape, kind),
+            pltpu.VMEM(up_weight.shape, kind),
+            pltpu.VMEM(down_weight.shape, kind),
+            pltpu.VMEM((4, n, capacity, width), kind),
+            pltpu.VMEM((8 * capacity, gate_weight.shape[1]), kind),
+            pltpu.VMEM((4, n, capacity, width), kind),
             pltpu.VMEM((n, 2, half, width), kind),
             pltpu.VMEM((n, 2, half, width), kind),
             pltpu.VMEM((n, half, width), kind),
             pltpu.VMEM((n, half, width), kind),
             pltpu.VMEM((n, 2, half, width), kind),
             pltpu.VMEM((n, capacity, width), kind),
-            two, two, two, two, one, one, one, one, one, one, one, one,
-        ],
-        compiler_params=pltpu.CompilerParams(collective_id=1, has_side_effects=True),
-    )(partial_value)
+            pltpu.SemaphoreType.DMA((3,)),
+        ]
+        + [one] * 10
+        + [two] * 4
+        + [one] * 8,
+        compiler_params=pltpu.CompilerParams(
+            collective_id=0, has_side_effects=True, vmem_limit_bytes=56 * 1024 * 1024
+        ),
+    )(sending, gate_weight, up_weight, down_weight)
 
 
 def project_kernel(x_ref, w_ref, out_ref, buf, acc, cols, gs, gr, as_, ar):
@@ -382,7 +403,12 @@
 ):
     attention = attend_local(queries, keys, values, sink_logit)
     capacity = max(2, 4 * residual.shape[0] // lax.axis_size("sp"))
-    in_plane = lax.axis_size("tp") == 4 and capacity % 32 == 0
+    in_plane = (
+        lax.axis_size("tp") == 4
+        and lax.axis_size("sp") == 8
+        and capacity % 32 == 0
+        and gate_weight.shape[2] % 256 == 0
+    )
     if in_plane:
         projected = project(attention, out_weight)
     else:
@@ -419,7 +445,7 @@
     )
     sending = sending.astype(jnp.bfloat16).reshape(sp_count, capacity, width)
     if in_plane:
-        piece = dispatch(sending)
+        returned = experts(sending, gate_weight[0], up_weight[0], down_weight[0])
     else:
         piece = lax.all_gather(
             lax.all_to_all(sending, "sp", split_axis=0, concat_axis=0, tiled=True),
@@ -427,18 +453,16 @@
             axis=0,
             tiled=True,
         )
-    flat = piece.reshape(-1, piece.shape[-1])
-    gate = jnp.dot(flat, gate_weight[0], preferred_element_type=jnp.float32)
-    upward = jnp.dot(flat, up_weight[0], preferred_element_type=jnp.float32)
-    hidden = (jax.nn.silu(gate) * upward).astype(jnp.bfloat16)
-    partial_value = jnp.dot(hidden, down_weight[0], preferred_element_type=jnp.float32)
-    partial_value = partial_value.reshape(piece.shape[:-1] + (down_weight.shape[-1],))
-    partial_value = partial_value.astype(jnp.bfloat16)
-    if in_plane:
-        returned = give_back(partial_value)
-    else:
+        flat = piece.reshape(-1, piece.shape[-1])
+        gate = jnp.dot(flat, gate_weight[0], preferred_element_type=jnp.float32)
+        upward = jnp.dot(flat, up_weight[0], preferred_element_type=jnp.float32)
+        hidden = (jax.nn.silu(gate) * upward).astype(jnp.bfloat16)
+        partial_value = jnp.dot(hidden, down_weight[0], preferred_element_type=jnp.float32)
+        partial_value = partial_value.reshape(piece.shape[:-1] + (down_weight.shape[-1],))
         returned = lax.all_to_all(
-            lax.psum_scatter(partial_value, "tp", scatter_dimension=0, tiled=True),
+            lax.psum_scatter(
+                partial_value.astype(jnp.bfloat16), "tp", scatter_dimension=0, tiled=True
+            ),
             "sp",
             split_axis=0,
             concat_axis=0,

time: 168 us -> 135 us (0.80)
  matrix products: 32 us -> 6.91 us
  Pallas kernels: 119 us -> 111 us
    dot_general x3 -> x0, matrix products: 25.1 us -> none  [the longest x1 9.04 us: local(): upward = jnp.dot(flat, up_weight[0], preferred_element_type=jnp.float32)]
    pallas_call x2 -> x1, Pallas kernels: 98.5 us -> 90.8 us  [experts(): pl.pallas_call(expert_kernel, out_shape=jax.ShapeDtypeStruct((n, capacity...]
  transfers between devices with their start and end apart: 2 -> 2, of which waited for: 0 -> 0; matrix products, arithmetic and copies ran while one was open for 3% -> 4% of each run, Pallas kernels for 0% -> 0%
where the time goes in v3:
time: 135 us; the launch traced here: 134 us
  Pallas kernels  111 us (82%)
  local copies, waits for them, and re-layouts  8.59 us (6%)
  matrix products  6.91 us (5%)
  starting transfers between devices  3.7 us (3%)
  other arithmetic  3.67 us (3%)
    pallas_call x1, Pallas kernels, experts(): pl.pallas_call(expert_kernel, out_shape=jax.ShapeDtypeStruct((n, capacity...  90.8 us
    pallas_call x1, Pallas kernels, project(): pl.pallas_call(project_kernel, out_shape=jax.ShapeDtypeStruct((2, 4, rows...  20.4 us
  transfers between devices with their start and end apart: 2, of which 0 were waited for; matrix products, arithmetic and copies ran while one was open for 4% of the time, Pallas kernels for 0%

profile of v3, /device:TPU:0, one launch (start us, length us, event | category | flops | bytes accessed | tf_op | source)
XLA Modules:
  0.0 134.2 jit_solution(10517487567614891137)
XLA Ops:
  0.0 0.9 constant_dynamic-update-slice_fusion.1
  0.9 0.9 constant_dynamic-update-slice_fusion
  1.9 2.4 %collective-permute-start = (bf16[128,512]{1,0:T(8,128)(2,1)S(1)}, bf16[128,512]{1,0:T(8,128)(2,1)S(1)}, u32[]{:S(2)}, u32[]{:S(2)}) collective-permute-start(bf16[128,512]{1,0:T(8,128)(2,1)S(1)} %get-tuple-element.9), channel_id=1, source_target_pairs={{0,4},{4,8},{8,12},{12,16},{16,20},{20,24},{24,28},{1,5},{5,9},{9,... | collective-permute-start | bytes 393224 | tf_op jit(solution)/shard_map/ppermute | solution.py:338
  4.3 1.3 collective-permute-start.1
  5.6 0.2 copy.36
  5.9 1.3 reshape.158
  7.2 0.7 max.18
  7.9 0.8 copy.44
  8.7 0.1 eq.30
  8.9 0.2 reduce_window_sum.11
  9.1 0.2 select_reduce_fusion
  9.3 0.1 reduce_sum.31
  9.5 0.7 multiply_add_fusion
  10.3 0.2 broadcast_and_fusion
  10.5 0.8 slice_bitcast_fusion.4
  11.3 0.2 copy.37
  11.5 0.2 copy.35
  11.6 0.1 pad_maximum_fusion
  11.8 0.7 fusion.1
  12.6 0.7 fusion
  13.4 1.0 fusion.7
  14.3 0.4 copy.51
  14.8 1.0 reshape.159.x_ref
  15.8 20.4 %shard_map.118 = bf16[2,4,64,256]{3,2,1,0:T(8,128)(2,1)} custom-call(bf16[256,512]{1,0:T(8,128)(2,1)} %reshape.159.x_ref, bf16[2048,512]{1,0:T(8,128)(2,1)} %w_ref.1), custom_call_target="tpu_custom_call" | custom-call | tf_op jit(solution)/shard_map/pallas_call | solution.py:314
  36.2 1.0 convert_bitcast_fusion
  37.2 0.4 copy.43
  37.6 0.4 reshape.155
  38.0 0.2 multiply_reduce_fusion
  38.2 1.5 %convolution_convert_fusion = bf16[256,2048]{1,0:T(8,128)(2,1)} fusion(f32[2048]{0:T(1024)S(1)} %copy-done.1, f32[64]{0:T(128)S(1)} %add_rsqrt_fusion, f32[64,2048]{1,0:T(8,128)S(1)} %reshape.155, bf16[64,2048]{1,0:T(8,128)(2,1)S(1)} %copy-done, bf16[64,2,256]{2,0,1:T(8,128)(2,1)S(1)} %get-tuple-element.14), kind=kOutput, calls=%fused_computation.4 | convolution fusion | flops 68304896 | bytes 1908992 | tf_op jit(solution)/shard_map/ts,td->sd/dot_general | solution.py:443
  39.7 90.8 %shard_map.119 = bf16[8,32,2048]{2,1,0:T(8,128)(2,1)} custom-call(bf16[8,32,2048]{2,1,0:T(8,128)(2,1)} %bitcast.57, bf16[2048,1280]{1,0:T(8,128)(2,1)} %bitcast.54, bf16[2048,1280]{1,0:T(8,128)(2,1)} %bitcast.55, bf16[1280,2048]{1,0:T(8,128)(2,1)} %bitcast.56), custom_call_target="tpu_custom_call" | custom-call | tf_op jit(solution)/shard_map/pallas_call | solution.py:221
  130.5 1.5 %convolution_multiply_fusion.1 = f32[64,2048]{1,0:T(8,128)S(1)} fusion(bf16[256,2048]{1,0:T(8,128)(2,1)} %bitcast.52, f32[64]{0:T(128)S(1)} %get-tuple-element.12, pred[64,2,256]{2,0,1:T(32,128)(4,1)S(1)} %get-tuple-element.13), kind=kOutput, calls=%fused_computation.8 | convolution fusion | flops 67239936 | bytes 1589760 | tf_op jit(solution)/shard_map/dot_general | solution.py:472
  132.0 2.2 %fusion.4 = bf16[64,2048]{1,0:T(8,128)(2,1)} fusion(f32[64,2048]{1,0:T(8,128)S(1)} %convolution_multiply_fusion.1, bf16[256,2048]{1,0:T(8,128)(2,1)} %bitcast.53, f32[64]{0:T(128)S(1)} %get-tuple-element.11, f32[64,2048]{1,0:T(8,128)S(1)} %reshape.155, bf16[64,2048]{1,0:T(8,128)(2,1)S(1)} %copy-done, pred[64,2,256]{2,0,1:T(32,128)(4,1)S(1)} %get-tuple-element.13), kind=kOutput, calls=%fused_computation.10 | convolution fusion | flops 67895296 | bytes 2638336 | tf_op jit(solution)/shard_map/dot_general | solution.py:473
  (19 shorter events, 0.7 us)
Async XLA Ops:
  1.9 9.4 %collective-permute-start = (bf16[128,512]{1,0:T(8,128)(2,1)S(1)}, bf16[128,512]{1,0:T(8,128)(2,1)S(1)}, u32[]{:S(2)}, u32[]{:S(2)}) collective-permute-start(bf16[128,512]{1,0:T(8,128)(2,1)S(1)} %get-tuple-element.9), channel_id=1, source_target_pairs={{0,4},{4,8},{8,12},{12,16},{16,20},{20,24},{24,28},{1,5},{5,9},{9,... | collective-permute-start | bytes 393224 | tf_op jit(solution)/shard_map/ppermute | solution.py:338
  4.3 7.0 %collective-permute-start.1 = (bf16[128,512]{1,0:T(8,128)(2,1)S(1)}, bf16[128,512]{1,0:T(8,128)(2,1)S(1)}, u32[]{:S(2)}, u32[]{:S(2)}) collective-permute-start(bf16[128,512]{1,0:T(8,128)(2,1)S(1)} %get-tuple-element.10), channel_id=1, source_target_pairs={{4,0},{8,4},{12,8},{16,12},{20,16},{24,20},{28,24},{5,1},{9,5},{13... | collective-permute-start | bytes 393224 | tf_op jit(solution)/shard_map/ppermute | solution.py:341
  14.8 23.2 %copy-start = (bf16[64,2048]{1,0:T(8,128)(2,1)S(1)}, bf16[64,2048]{1,0:T(8,128)(2,1)}, u32[]{:S(2)}) copy-start(bf16[64,2048]{1,0:T(8,128)(2,1)} %param.17) | copy-start | bytes 786436
  15.8 22.4 %copy-start.1 = (f32[2048]{0:T(1024)S(1)}, f32[2048]{0:T(1024)}, u32[]{:S(2)}) copy-start(f32[2048]{0:T(1024)} %param.18) | copy-start | bytes 24580
